TPU v7x, 32 devices: a whole 2x2x4 slice. The times are simulated.
32 devices in a mesh: grp: 2 (over y), dp: 2 (over x), kv: 4 (over z), tp: 2 (over core).
Axes of the slice: x: 2, y: 2, z: 4, core: 2. Of those that a mesh axis runs over, the one named last changes fastest.
Arguments:
- tokens: bfloat16 [32, 2048], P(('grp', 'dp'), ('kv', 'tp')), parts along dimension 0, may hold values from -24 to 24
- memory: float32 [32, 12, 16384], P(('grp', 'dp', 'kv', 'tp')), parts along dimension 0, may hold values from -3 to 3
- mix_gain: float32 [2048], replicated, may hold values from 0.1 to 1.9
- w_query: bfloat16 [2048, 1536], P(None, ('kv', 'tp')), may hold values from -0.125 to 0.125
- w_key: bfloat16 [2048, 1536], P(None, ('kv', 'tp')), may hold values from -0.125 to 0.125
- w_value: bfloat16 [2048, 1536], P(None, ('kv', 'tp')), may hold values from -0.125 to 0.125
- w_gate: bfloat16 [2048, 1536], P(None, ('kv', 'tp')), may hold values from -0.125 to 0.125
- w_beta: bfloat16 [2048, 12], replicated, may hold values from -0.125 to 0.125
- w_decay: bfloat16 [2048, 12], replicated, may hold values from -0.125 to 0.125
- decay_rate: float32 [12], replicated, may hold values from 0.1 to 3
- decay_bias: float32 [12], replicated, may hold values from -2 to 1
- head_gain: float32 [128], replicated, may hold values from 0.1 to 1.9
- w_out: bfloat16 [1536, 2048], P(None, ('kv', 'tp')), may hold values from -0.15625 to 0.15625
- ffn_gain: float32 [2048], replicated, may hold values from 0.1 to 1.9
- w_up: bfloat16 [2048, 8192], P(None, ('kv', 'tp')), may hold values from -0.125 to 0.125
- w_down: bfloat16 [8192, 2048], P(('kv', 'tp')), may hold values from -0.09375 to 0.09375
Outputs:
- layer_out: bfloat16 [32, 2048], P(('grp', 'dp'), ('kv', 'tp')), parts along dimension 0
- new_memory: float32 [32, 12, 16384], P(('grp', 'dp', 'kv', 'tp')), parts along dimension 0
There are 2 independent parts, one for each index of `grp`. A program takes and returns all parts, laid end to end along the dimension named above; an argument that names none is the same for every part. Nothing has to cross between parts.
All inputs are finite; a program needn't handle non-finite values.
Results may differ from a plain program's by a relative error of at most 0.02.
Values may be sent and summed in bfloat16 or wider, within the bound.
A program may use at most 64 MiB of HBM per device.

v0:
```python
import jax
import jax.numpy as jnp
from jax import lax
from jax.sharding import PartitionSpec as P

epsilon = 1e-06


def shortened(value):
    return jax.tree.map(lambda a: a.astype(jnp.bfloat16) if a.dtype == jnp.float32 else a, value)


def delta_step(queries, keys_in, values, gates, strength, log_decay, memory, head_gain):
    count = queries.shape[0]
    heads = strength.shape[1]
    size = head_gain.shape[0]
    highest = lax.Precision.HIGHEST
    query_wide = queries.astype(jnp.float32).reshape(count, heads, size)
    key_wide = keys_in.astype(jnp.float32).reshape(count, heads, size)
    value_wide = values.astype(jnp.float32).reshape(count, heads, size)
    gate_wide = gates.astype(jnp.float32).reshape(count, heads, size)
    unit_key = key_wide * lax.rsqrt(jnp.sum(key_wide * key_wide, axis=-1, keepdims=True) + epsilon)
    matrix = memory.reshape(count, heads, size, size)
    recall = jnp.einsum("bhk,bhkv->bhv", unit_key, matrix, precision=highest)
    retain = jnp.exp(log_decay)[:, :, None, None]
    scaled = strength[:, :, None]
    erased = matrix - jnp.einsum("bhk,bhv->bhkv", unit_key, scaled * recall, precision=highest)
    written = jnp.einsum("bhk,bhv->bhkv", unit_key, scaled * value_wide, precision=highest)
    updated = retain * erased + written
    readout = jnp.einsum("bhk,bhkv->bhv", query_wide, updated, precision=highest)
    normed = readout * lax.rsqrt(jnp.mean(readout * readout, axis=-1, keepdims=True) + epsilon)
    normed = normed * head_gain * jax.nn.silu(gate_wide)
    return (
        updated.reshape(count, heads, size * size),
        normed.reshape(count, heads * size).astype(jnp.bfloat16),
    )


def per_device(
    tokens,
    memory,
    mix_gain,
    w_query,
    w_key,
    w_value,
    w_gate,
    w_beta,
    w_decay,
    decay_rate,
    decay_bias,
    head_gain,
    w_out,
    ffn_gain,
    w_up,
    w_down,
):
    rows = tokens.shape[0]
    owned = memory.shape[0]
    width = mix_gain.shape[0]
    lane = lax.axis_index(("kv", "tp"))
    own_start = lane * owned
    wide = tokens.astype(jnp.float32)
    head_weights = (w_query, w_key, w_value, w_gate)
    small_weights = (w_beta, w_decay)

    def fold_proj(carry, piece, start):
        mine = lax.dynamic_slice_in_dim(piece, own_start, owned, 0)
        large = tuple(
            (jnp.dot(piece, weight, preferred_element_type=jnp.float32) for weight in head_weights)
        )
        small = tuple(
            (jnp.dot(mine, weight, preferred_element_type=jnp.float32) for weight in small_weights)
        )
        return large + small

    def fold_up(total, piece, start):
        return jnp.dot(piece, w_up, preferred_element_type=jnp.float32)

    def with_squares(inner, gain, carry, piece, start):
        piece_wide = piece.astype(jnp.float32)
        lifted = (piece_wide * gain).astype(jnp.bfloat16)
        return (inner(carry[0], lifted, start), jnp.sum(piece_wide * piece_wide, axis=1))

    proj_init = tuple((jnp.zeros((rows, weight.shape[1]), jnp.float32) for weight in head_weights))
    proj_init = proj_init + tuple(
        (jnp.zeros((owned, weight.shape[1]), jnp.float32) for weight in small_weights)
    )
    row_zeros = jnp.zeros((rows,), jnp.float32)
    folded, total_in = with_squares(
        fold_proj,
        mix_gain,
        (proj_init, row_zeros),
        lax.all_gather(tokens, ("kv", "tp"), axis=1, tiled=True),
        jnp.int32(0),
    )
    scale_in = lax.rsqrt(total_in / width + epsilon)
    sent = tuple(((total * scale_in[:, None]).astype(jnp.bfloat16) for total in folded[:4]))
    scale_own = lax.dynamic_slice_in_dim(scale_in, own_start, owned)[:, None]
    strength = jax.nn.sigmoid(folded[4] * scale_own)
    log_decay = -decay_rate * jax.nn.softplus(folded[5] * scale_own + decay_bias)
    queries, keys_in, values, gates = jax.tree.map(
        lambda part, own: part.astype(own.dtype),
        lax.all_to_all(shortened(sent), ("kv", "tp"), split_axis=0, concat_axis=1, tiled=True),
        sent,
    )
    updated, mixed = delta_step(
        queries, keys_in, values, gates, strength, log_decay, memory, head_gain
    )
    branch = jnp.dot(
        lax.all_gather(mixed, ("kv", "tp"), axis=0, tiled=True),
        w_out,
        preferred_element_type=jnp.float32,
    )
    middle = (wide + branch).astype(jnp.bfloat16)
    middle_wide = middle.astype(jnp.float32)
    up_init = jnp.zeros((rows, w_up.shape[1]), jnp.float32)
    raised, total_mid = with_squares(
        fold_up,
        ffn_gain,
        (up_init, row_zeros),
        lax.all_gather(middle, ("kv", "tp"), axis=1, tiled=True),
        jnp.int32(0),
    )
    scale_mid = lax.rsqrt(total_mid / width + epsilon)[:, None]
    hidden = jnp.square(jax.nn.relu(raised * scale_mid)).astype(jnp.bfloat16)
    terms = jnp.dot(hidden, w_down, preferred_element_type=jnp.float32)
    down = lax.psum_scatter(
        terms.astype(jnp.bfloat16), ("kv", "tp"), scatter_dimension=1, tiled=True
    ).astype(jnp.float32)
    layer_out = (middle_wide + down).astype(jnp.bfloat16)
    return (layer_out, updated)


def solution(mesh):
    placed = (
        P(("grp", "dp"), ("kv", "tp")),
        P(("grp", "dp", "kv", "tp"), None, None),
        P(),
        P(None, ("kv", "tp")),
        P(None, ("kv", "tp")),
        P(None, ("kv", "tp")),
        P(None, ("kv", "tp")),
        P(),
        P(),
        P(),
        P(),
        P(),
        P(None, ("kv", "tp")),
        P(),
        P(None, ("kv", "tp")),
        P(("kv", "tp"), None),
    )
    return jax.shard_map(
        per_device,
        mesh=mesh,
        in_specs=placed,
        out_specs=(P(("grp", "dp"), ("kv", "tp")), P(("grp", "dp", "kv", "tp"), None, None)),
        check_vma=False,
    )
```

profile of v0, /device:TPU:0, one launch (start us, length us, event | category | flops | bytes accessed | tf_op | source)
XLA Modules:
  0.0 142.1 jit_solution(9691909267525715545)
XLA Ops:
  7.2 16.1 %all_gather.9 = bf16[8,2048]{1,0:T(8,128)(2,1)S(1)} all-gather(bf16[8,256]{1,0:T(8,128)(2,1)} %param.16), channel_id=1, replica_groups=mesh['grp'=2,'dp'=2,'kv'=4,'tp'=2] {'kv','tp'}, dimensions={1}, use_global_device_ids=true | all-gather | bytes 36864 | tf_op jit(solution)/shard_map/all_gather | solution.py:93
  23.3 0.8 fusion.20
  24.1 1.4 %fusion.10 = bf16[8,1,192]{2,0,1:T(8,128)(2,1)S(1)} fusion(bf16[8,2048]{1,0:T(8,128)(2,1)S(1)} %get-tuple-element.5, bf16[2048,192]{0,1:T(8,128)(2,1)} %param.20, f32[8]{0:T(128)S(1)} %add_rsqrt_fusion.3), kind=kOutput, calls=%fused_computation.17 | convolution fusion | flops 6294528 | bytes 822304 | tf_op jit(solution)/shard_map/dot_general | solution.py:69
  25.6 0.6 copy.23
  26.2 4.6 %all-to-all-start.1 = ((bf16[8,1,192]{2,1,0:T(2,128)(2,1)}), bf16[8,1,192]{2,1,0:T(2,128)(2,1)S(1)}, u32[]{:S(2)}, u32[]{:S(2)}) async-start(bf16[8,1,192]{2,1,0:T(2,128)(2,1)} %copy.23), calls=%async_computation.1 | async-start | bytes 16384 | tf_op jit(solution)/shard_map/all_to_all | solution.py:103
  30.8 0.6 dynamic_slice.7
  31.4 1.4 %fusion.9 = bf16[8,1,192]{2,0,1:T(8,128)(2,1)S(1)} fusion(bf16[8,2048]{1,0:T(8,128)(2,1)S(1)} %get-tuple-element.5, bf16[2048,192]{0,1:T(8,128)(2,1)} %param.21, f32[8]{0:T(128)S(1)} %add_rsqrt_fusion.3), kind=kOutput, calls=%fused_computation.16 | convolution fusion | flops 6294528 | bytes 822304 | tf_op jit(solution)/shard_map/dot_general | solution.py:69
  32.8 1.5 %fusion.8 = bf16[8,1,192]{2,0,1:T(8,128)(2,1)S(1)} fusion(bf16[8,2048]{1,0:T(8,128)(2,1)S(1)} %get-tuple-element.5, bf16[2048,192]{0,1:T(8,128)(2,1)} %param.22, f32[8]{0:T(128)S(1)} %add_rsqrt_fusion.3), kind=kOutput, calls=%fused_computation.15 | convolution fusion | flops 6294528 | bytes 822304 | tf_op jit(solution)/shard_map/dot_general | solution.py:69
  34.3 1.6 %fusion.16 = f32[12]{0:T(128)S(1)} fusion(bf16[2048,12]{0,1:T(8,128)(2,1)} %param.23, bf16[8,2048]{1,0:T(8,128)(2,1)S(1)} %get-tuple-element.5, s32[]{:T(128)S(6)} %select_n.9, f32[]{:T(128)} %bitcast.2), kind=kOutput, calls=%fused_computation.24 | convolution fusion | flops 49200 | bytes 57400 | tf_op jit(solution)/shard_map/dot_general | solution.py:72
  35.9 1.7 %fusion.45 = f32[12]{0:T(128)S(1)} fusion(f32[12]{0:T(128)} %param.26, bf16[2048,12]{0,1:T(8,128)(2,1)} %param.24, bf16[8,2048]{1,0:T(8,128)(2,1)S(1)} %get-tuple-element.5, s32[]{:T(128)S(6)} %select_n.9, f32[12]{0:T(128)} %param.25, f32[]{:T(128)} %bitcast.2), kind=kOutput, calls=%fused_computation.68 | convolution fusion | flops 49272 | bytes 57496 | tf_op jit(solution)/shard_map/dot_general | solution.py:72
  37.6 1.5 %fusion.11 = bf16[8,1,192]{2,0,1:T(8,128)(2,1)S(1)} fusion(bf16[8,2048]{1,0:T(8,128)(2,1)S(1)} %get-tuple-element.5, bf16[2048,192]{0,1:T(8,128)(2,1)} %param.19, f32[8]{0:T(128)S(1)} %add_rsqrt_fusion.3), kind=kOutput, calls=%fused_computation.18 | convolution fusion | flops 6294528 | bytes 822304 | tf_op jit(solution)/shard_map/dot_general | solution.py:69
  39.0 0.6 copy.24
  39.7 0.6 copy.22
  40.3 0.6 copy.25
  40.9 5.1 %all-to-all-start.3 = ((bf16[8,1,192]{2,1,0:T(2,128)(2,1)}), bf16[8,1,192]{2,1,0:T(2,128)(2,1)S(1)}, u32[]{:S(2)}, u32[]{:S(2)}) async-start(bf16[8,1,192]{2,1,0:T(2,128)(2,1)} %copy.25), calls=%async_computation.3 | async-start | bytes 16384 | tf_op jit(solution)/shard_map/all_to_all | solution.py:103
  46.1 0.1 reduce_sum.37
  46.4 5.2 %all-to-all-done.3 = bf16[8,1,192]{2,1,0:T(2,128)(2,1)S(1)} async-done(((bf16[8,1,192]{2,1,0:T(2,128)(2,1)}), bf16[8,1,192]{2,1,0:T(2,128)(2,1)S(1)}, u32[]{:S(2)}, u32[]{:S(2)}) %all-to-all-start.3) | async-done | bytes 3104 | tf_op jit(solution)/shard_map/all_to_all | solution.py:103
  51.6 3.3 %all-to-all-start = ((bf16[8,1,192]{2,1,0:T(2,128)(2,1)}), bf16[8,1,192]{2,1,0:T(2,128)(2,1)S(1)}, u32[]{:S(2)}, u32[]{:S(2)}) async-start(bf16[8,1,192]{2,1,0:T(2,128)(2,1)} %copy.22), calls=%async_computation | async-start | bytes 16384 | tf_op jit(solution)/shard_map/all_to_all | solution.py:103
  55.0 5.5 %all-to-all-done = bf16[8,1,192]{2,1,0:T(2,128)(2,1)S(1)} async-done(((bf16[8,1,192]{2,1,0:T(2,128)(2,1)}), bf16[8,1,192]{2,1,0:T(2,128)(2,1)S(1)}, u32[]{:S(2)}, u32[]{:S(2)}) %all-to-all-start) | async-done | bytes 3104 | tf_op jit(solution)/shard_map/all_to_all | solution.py:103
  60.5 3.3 %all-to-all-start.2 = ((bf16[8,1,192]{2,1,0:T(2,128)(2,1)}), bf16[8,1,192]{2,1,0:T(2,128)(2,1)S(1)}, u32[]{:S(2)}, u32[]{:S(2)}) async-start(bf16[8,1,192]{2,1,0:T(2,128)(2,1)} %copy.24), calls=%async_computation.2 | async-start | bytes 16384 | tf_op jit(solution)/shard_map/all_to_all | solution.py:103
  64.1 5.3 %all-to-all-done.2 = bf16[8,1,192]{2,1,0:T(2,128)(2,1)S(1)} async-done(((bf16[8,1,192]{2,1,0:T(2,128)(2,1)}), bf16[8,1,192]{2,1,0:T(2,128)(2,1)S(1)}, u32[]{:S(2)}, u32[]{:S(2)}) %all-to-all-start.2) | async-done | bytes 3104 | tf_op jit(solution)/shard_map/all_to_all | solution.py:103
  69.5 0.8 fusion.38
  70.3 0.3 multiply_add_fusion
  70.6 0.5 fusion.51
  71.1 0.1 fusion.33
  71.3 14.0 %all-gather = bf16[8,1,1536]{2,1,0:T(2,128)(2,1)S(1)} all-gather(bf16[1,1,1536]{2,1,0:T(2,128)(2,1)S(1)} %reshape.232), channel_id=1, replica_groups=mesh['grp'=2,'dp'=2,'kv'=4,'tp'=2] {'kv','tp'}, dimensions={0}, use_global_device_ids=true | all-gather | bytes 27648 | tf_op jit(solution)/shard_map/all_gather | solution.py:110
  85.3 0.2 fusion.7
  85.5 14.1 %all_gather.11 = bf16[8,2048]{1,0:T(8,128)(2,1)S(1)} all-gather(bf16[8,256]{1,0:T(8,128)(2,1)S(1)} %fusion.7), channel_id=1, replica_groups=mesh['grp'=2,'dp'=2,'kv'=4,'tp'=2] {'kv','tp'}, dimensions={1}, use_global_device_ids=true | all-gather | bytes 36864 | tf_op jit(solution)/shard_map/all_gather | solution.py:121
  99.6 0.1 fusion.22
  99.8 5.3 %convolution_convert_fusion = bf16[8,2048]{1,0:T(8,128)(2,1)} fusion(bf16[1024,2048]{1,0:T(8,128)(2,1)} %param.31, bf16[2048,1024]{1,0:T(8,128)(2,1)} %param.30, bf16[8,2048]{1,0:T(8,128)(2,1)S(1)} %all_gather.11, f32[2048]{0:T(1024)S(1)} %copy-done.4, f32[8]{0:T(128)S(1)} %add_rsqrt_fusion), kind=kOutput, calls=%fused_computation | convolution fusion | flops 67207168 | bytes 8462368 | tf_op jit(solution)/shard_map/dot_general | solution.py:126
  105.1 28.9 %reduce-scatter.2.cloned.1.call-done = bf16[8,256]{1,0:T(8,128)(2,1)} async-done(((bf16[8,2048]{1,0:T(8,128)(2,1)}), bf16[8,256]{1,0:T(8,128)(2,1)}) %reduce-scatter.2.cloned.1.call-update) | async-done | bytes 4112 | tf_op jit(solution)/shard_map/reduce_scatter | solution.py:127
  134.0 1.3 add_convert_fusion
  (33 shorter events, 0.9 us)
Async XLA Ops:
  7.2 78.2 %copy-start = (bf16[1536,256]{1,0:T(8,128)(2,1)S(1)}, bf16[1536,256]{1,0:T(8,128)(2,1)}, u32[]{:S(2)}) copy-start(bf16[1536,256]{1,0:T(8,128)(2,1)} %param.28) | copy-start | bytes 2359300
  7.2 78.2 %copy-start.3 = (bf16[8,256]{1,0:T(8,128)(2,1)S(1)}, bf16[8,256]{1,0:T(8,128)(2,1)}, u32[]{:S(2)}) copy-start(bf16[8,256]{1,0:T(8,128)(2,1)} %param.16) | copy-start | bytes 12292
  7.2 62.3 %copy-start.1 = (f32[1,12,16384]{2,0,1:T(1,128)S(1)}, f32[1,12,16384]{2,0,1:T(1,128)}, u32[]{:S(2)}) copy-start(f32[1,12,16384]{2,0,1:T(1,128)} %param.17) | copy-start | bytes 2359300
  7.2 64.0 %copy-start.5 = (f32[128]{0:T(128)S(1)}, f32[128]{0:T(128)}, u32[]{:S(2)}) copy-start(f32[128]{0:T(128)} %param.27) | copy-start | bytes 1540
  7.2 92.6 %copy-start.4 = (f32[2048]{0:T(1024)S(1)}, f32[2048]{0:T(1024)}, u32[]{:S(2)}) copy-start(f32[2048]{0:T(1024)} %param.29) | copy-start | bytes 24580
  26.2 14.7 %all-to-all-start.1 = ((bf16[8,1,192]{2,1,0:T(2,128)(2,1)}), bf16[8,1,192]{2,1,0:T(2,128)(2,1)S(1)}, u32[]{:S(2)}, u32[]{:S(2)}) async-start(bf16[8,1,192]{2,1,0:T(2,128)(2,1)} %copy.23), calls=%async_computation.1 | async-start | bytes 16384 | tf_op jit(solution)/shard_map/all_to_all | solution.py:103
  40.9 10.7 %all-to-all-start.3 = ((bf16[8,1,192]{2,1,0:T(2,128)(2,1)}), bf16[8,1,192]{2,1,0:T(2,128)(2,1)S(1)}, u32[]{:S(2)}, u32[]{:S(2)}) async-start(bf16[8,1,192]{2,1,0:T(2,128)(2,1)} %copy.25), calls=%async_computation.3 | async-start | bytes 16384 | tf_op jit(solution)/shard_map/all_to_all | solution.py:103
  51.6 8.9 %all-to-all-start = ((bf16[8,1,192]{2,1,0:T(2,128)(2,1)}), bf16[8,1,192]{2,1,0:T(2,128)(2,1)S(1)}, u32[]{:S(2)}, u32[]{:S(2)}) async-start(bf16[8,1,192]{2,1,0:T(2,128)(2,1)} %copy.22), calls=%async_computation | async-start | bytes 16384 | tf_op jit(solution)/shard_map/all_to_all | solution.py:103
  60.5 8.9 %all-to-all-start.2 = ((bf16[8,1,192]{2,1,0:T(2,128)(2,1)}), bf16[8,1,192]{2,1,0:T(2,128)(2,1)S(1)}, u32[]{:S(2)}, u32[]{:S(2)}) async-start(bf16[8,1,192]{2,1,0:T(2,128)(2,1)} %copy.24), calls=%async_computation.2 | async-start | bytes 16384 | tf_op jit(solution)/shard_map/all_to_all | solution.py:103
  63.8 70.2 %reduce-scatter.2.cloned.1.call-start = ((), (), s32[]{:S(2)}) async-start(), calls=%async_computation.5 | async-start | bytes 36864 | tf_op jit(solution)/shard_map/reduce_scatter | solution.py:127
  70.6 34.5 %copy-start.2 = (f32[12,128,128]{2,1,0:T(8,128)}, f32[12,128,128]{2,1,0:T(8,128)S(1)}, u32[]{:S(2)}) copy-start(f32[12,128,128]{2,1,0:T(8,128)S(1)} %multiply_add_fusion) | copy-start | bytes 2359300
Sparse Core Ops, SparseCore 0:
  105.2 28.7 reduce-scatter.1
where the time goes:
time: 143 us; the launch traced here: 142 us
  waiting for transfers between devices  44.9 us (31%)
  blocking collectives  44.2 us (31%)
  starting transfers between devices  16.4 us (11%)
  matrix products  15.8 us (11%)
  between operations  14.2 us (10%)
  local copies, waits for them, and re-layouts  3.45 us (2%)
  other arithmetic  3.2 us (2%)
    reduce_scatter x1, waiting for transfers between devices, per_device(): lax.psum_scatter(terms.astype(jnp.bfloat16), ('kv', 'tp'), scatter_dimens...  28.9 us
    all_to_all x4, starting transfers between devices, per_device(): lax.all_to_all(shortened(sent), ('kv', 'tp'), split_axis=0, concat_axis=1...  16.4 us
    all_gather x1, blocking collectives, per_device(): lax.all_gather(tokens, ('kv', 'tp'), axis=1, tiled=True)  16.1 us
    all_to_all x4, waiting for transfers between devices, per_device(): lax.all_to_all(shortened(sent), ('kv', 'tp'), split_axis=0, concat_axis=1...  15.9 us
    all_gather x1, blocking collectives, per_device(): lax.all_gather(middle, ('kv', 'tp'), axis=1, tiled=True)  14.1 us
    all_gather x1, blocking collectives, per_device(): lax.all_gather(mixed, ('kv', 'tp'), axis=0, tiled=True)  14 us
    dot_general x4, matrix products, fold_proj(): jnp.dot(piece, weight, preferred_element_type=jnp.float32)  5.79 us
    dot_general x1, matrix products, per_device(): terms = jnp.dot(hidden, w_down, preferred_element_type=jnp.float32)  5.28 us
  transfers between devices with their start and end apart: 5, of which 4 were waited for; matrix products, arithmetic and copies ran while one was open for 8% of the time, Pallas kernels for 0%

commit v1 on v0

--- a/solution.py
+++ b/solution.py
@@ -118,7 +118,7 @@
         fold_up,
         ffn_gain,
         (up_init, row_zeros),
-        lax.all_gather(middle, ("kv", "tp"), axis=1, tiled=True),
+        jnp.concatenate(lax.all_gather(middle, ("kv", "tp")), axis=1),
         jnp.int32(0),
     )
     scale_mid = lax.rsqrt(total_mid / width + epsilon)[:, None]

time: 143 us -> 143 us (level)
  no operation moved by 1% of the time
where the time goes in v1:
time: 143 us; the launch traced here: 142 us
  waiting for transfers between devices  44.9 us (31%)
  blocking collectives  44.2 us (31%)
  starting transfers between devices  16.4 us (11%)
  matrix products  15.8 us (11%)
  between operations  14.2 us (10%)
  local copies, waits for them, and re-layouts  3.45 us (2%)
  other arithmetic  3.21 us (2%)
    reduce_scatter x1, waiting for transfers between devices, per_device(): lax.psum_scatter(terms.astype(jnp.bfloat16), ('kv', 'tp'), scatter_dimens...  28.9 us
    all_to_all x4, starting transfers between devices, per_device(): lax.all_to_all(shortened(sent), ('kv', 'tp'), split_axis=0, concat_axis=1...  16.4 us
    all_gather x1, blocking collectives, per_device(): lax.all_gather(tokens, ('kv', 'tp'), axis=1, tiled=True)  16.1 us
    all_to_all x4, waiting for transfers between devices, per_device(): lax.all_to_all(shortened(sent), ('kv', 'tp'), split_axis=0, concat_axis=1...  15.9 us
    all_gather x1, blocking collectives, per_device(): lax.all_gather(middle, ('kv', 'tp'))  14.1 us
    all_gather x1, blocking collectives, per_device(): lax.all_gather(mixed, ('kv', 'tp'), axis=0, tiled=True)  14 us
    dot_general x4, matrix products, fold_proj(): jnp.dot(piece, weight, preferred_element_type=jnp.float32)  5.79 us
    dot_general x1, matrix products, per_device(): terms = jnp.dot(hidden, w_down, preferred_element_type=jnp.float32)  5.28 us
  transfers between devices with their start and end apart: 5, of which 4 were waited for; matrix products, arithmetic and copies ran while one was open for 8% of the time, Pallas kernels for 0%

profile of v1, /device:TPU:0, one launch (start us, length us, event | category | flops | bytes accessed | tf_op | source)
XLA Modules:
  0.0 142.1 jit_solution(15900982767679141224)
XLA Ops:
  7.2 16.1 %all_gather.12 = bf16[8,2048]{1,0:T(8,128)(2,1)S(1)} all-gather(bf16[8,256]{1,0:T(8,128)(2,1)} %param.16), channel_id=1, replica_groups=mesh['grp'=2,'dp'=2,'kv'=4,'tp'=2] {'kv','tp'}, dimensions={1}, use_global_device_ids=true | all-gather | bytes 36864 | tf_op jit(solution)/shard_map/all_gather | solution.py:93
  23.3 0.8 fusion.20
  24.1 1.4 %fusion.10 = bf16[8,1,192]{2,0,1:T(8,128)(2,1)S(1)} fusion(bf16[8,2048]{1,0:T(8,128)(2,1)S(1)} %get-tuple-element.5, bf16[2048,192]{0,1:T(8,128)(2,1)} %param.20, f32[8]{0:T(128)S(1)} %add_rsqrt_fusion.3), kind=kOutput, calls=%fused_computation.17 | convolution fusion | flops 6294528 | bytes 822304 | tf_op jit(solution)/shard_map/dot_general | solution.py:69
  25.6 0.6 copy.23
  26.2 4.6 %all-to-all-start.1 = ((bf16[8,1,192]{2,1,0:T(2,128)(2,1)}), bf16[8,1,192]{2,1,0:T(2,128)(2,1)S(1)}, u32[]{:S(2)}, u32[]{:S(2)}) async-start(bf16[8,1,192]{2,1,0:T(2,128)(2,1)} %copy.23), calls=%async_computation.1 | async-start | bytes 16384 | tf_op jit(solution)/shard_map/all_to_all | solution.py:103
  30.8 0.6 dynamic_slice.7
  31.4 1.4 %fusion.9 = bf16[8,1,192]{2,0,1:T(8,128)(2,1)S(1)} fusion(bf16[8,2048]{1,0:T(8,128)(2,1)S(1)} %get-tuple-element.5, bf16[2048,192]{0,1:T(8,128)(2,1)} %param.21, f32[8]{0:T(128)S(1)} %add_rsqrt_fusion.3), kind=kOutput, calls=%fused_computation.16 | convolution fusion | flops 6294528 | bytes 822304 | tf_op jit(solution)/shard_map/dot_general | solution.py:69
  32.8 1.5 %fusion.8 = bf16[8,1,192]{2,0,1:T(8,128)(2,1)S(1)} fusion(bf16[8,2048]{1,0:T(8,128)(2,1)S(1)} %get-tuple-element.5, bf16[2048,192]{0,1:T(8,128)(2,1)} %param.22, f32[8]{0:T(128)S(1)} %add_rsqrt_fusion.3), kind=kOutput, calls=%fused_computation.15 | convolution fusion | flops 6294528 | bytes 822304 | tf_op jit(solution)/shard_map/dot_general | solution.py:69
  34.3 1.6 %fusion.16 = f32[12]{0:T(128)S(1)} fusion(bf16[2048,12]{0,1:T(8,128)(2,1)} %param.23, bf16[8,2048]{1,0:T(8,128)(2,1)S(1)} %get-tuple-element.5, s32[]{:T(128)S(6)} %select_n.9, f32[]{:T(128)} %bitcast.2), kind=kOutput, calls=%fused_computation.24 | convolution fusion | flops 49200 | bytes 57400 | tf_op jit(solution)/shard_map/dot_general | solution.py:72
  35.9 1.7 %fusion.41 = f32[12]{0:T(128)S(1)} fusion(f32[12]{0:T(128)} %param.26, bf16[2048,12]{0,1:T(8,128)(2,1)} %param.24, bf16[8,2048]{1,0:T(8,128)(2,1)S(1)} %get-tuple-element.5, s32[]{:T(128)S(6)} %select_n.9, f32[12]{0:T(128)} %param.25, f32[]{:T(128)} %bitcast.2), kind=kOutput, calls=%fused_computation.67 | convolution fusion | flops 49272 | bytes 57496 | tf_op jit(solution)/shard_map/dot_general | solution.py:72
  37.6 1.5 %fusion.11 = bf16[8,1,192]{2,0,1:T(8,128)(2,1)S(1)} fusion(bf16[8,2048]{1,0:T(8,128)(2,1)S(1)} %get-tuple-element.5, bf16[2048,192]{0,1:T(8,128)(2,1)} %param.19, f32[8]{0:T(128)S(1)} %add_rsqrt_fusion.3), kind=kOutput, calls=%fused_computation.18 | convolution fusion | flops 6294528 | bytes 822304 | tf_op jit(solution)/shard_map/dot_general | solution.py:69
  39.0 0.6 copy.24
  39.7 0.6 copy.22
  40.3 0.6 copy.25
  40.9 5.1 %all-to-all-start.3 = ((bf16[8,1,192]{2,1,0:T(2,128)(2,1)}), bf16[8,1,192]{2,1,0:T(2,128)(2,1)S(1)}, u32[]{:S(2)}, u32[]{:S(2)}) async-start(bf16[8,1,192]{2,1,0:T(2,128)(2,1)} %copy.25), calls=%async_computation.3 | async-start | bytes 16384 | tf_op jit(solution)/shard_map/all_to_all | solution.py:103
  46.1 0.1 reduce_sum.37
  46.4 5.2 %all-to-all-done.3 = bf16[8,1,192]{2,1,0:T(2,128)(2,1)S(1)} async-done(((bf16[8,1,192]{2,1,0:T(2,128)(2,1)}), bf16[8,1,192]{2,1,0:T(2,128)(2,1)S(1)}, u32[]{:S(2)}, u32[]{:S(2)}) %all-to-all-start.3) | async-done | bytes 3104 | tf_op jit(solution)/shard_map/all_to_all | solution.py:103
  51.6 3.3 %all-to-all-start = ((bf16[8,1,192]{2,1,0:T(2,128)(2,1)}), bf16[8,1,192]{2,1,0:T(2,128)(2,1)S(1)}, u32[]{:S(2)}, u32[]{:S(2)}) async-start(bf16[8,1,192]{2,1,0:T(2,128)(2,1)} %copy.22), calls=%async_computation | async-start | bytes 16384 | tf_op jit(solution)/shard_map/all_to_all | solution.py:103
  55.0 5.5 %all-to-all-done = bf16[8,1,192]{2,1,0:T(2,128)(2,1)S(1)} async-done(((bf16[8,1,192]{2,1,0:T(2,128)(2,1)}), bf16[8,1,192]{2,1,0:T(2,128)(2,1)S(1)}, u32[]{:S(2)}, u32[]{:S(2)}) %all-to-all-start) | async-done | bytes 3104 | tf_op jit(solution)/shard_map/all_to_all | solution.py:103
  60.5 3.3 %all-to-all-start.2 = ((bf16[8,1,192]{2,1,0:T(2,128)(2,1)}), bf16[8,1,192]{2,1,0:T(2,128)(2,1)S(1)}, u32[]{:S(2)}, u32[]{:S(2)}) async-start(bf16[8,1,192]{2,1,0:T(2,128)(2,1)} %copy.24), calls=%async_computation.2 | async-start | bytes 16384 | tf_op jit(solution)/shard_map/all_to_all | solution.py:103
  64.1 5.3 %all-to-all-done.2 = bf16[8,1,192]{2,1,0:T(2,128)(2,1)S(1)} async-done(((bf16[8,1,192]{2,1,0:T(2,128)(2,1)}), bf16[8,1,192]{2,1,0:T(2,128)(2,1)S(1)}, u32[]{:S(2)}, u32[]{:S(2)}) %all-to-all-start.2) | async-done | bytes 3104 | tf_op jit(solution)/shard_map/all_to_all | solution.py:103
  69.5 0.8 fusion.34
  70.3 0.3 multiply_add_fusion
  70.6 0.5 fusion.47
  71.1 0.1 fusion.29
  71.3 14.0 %all-gather.1 = bf16[8,1,1536]{2,1,0:T(2,128)(2,1)S(1)} all-gather(bf16[1,1,1536]{2,1,0:T(2,128)(2,1)S(1)} %reshape.240), channel_id=1, replica_groups=mesh['grp'=2,'dp'=2,'kv'=4,'tp'=2] {'kv','tp'}, dimensions={0}, use_global_device_ids=true | all-gather | bytes 27648 | tf_op jit(solution)/shard_map/all_gather | solution.py:110
  85.3 0.2 fusion.7
  85.5 14.1 %all-gather = bf16[64,256]{1,0:T(8,128)(2,1)S(1)} all-gather(bf16[8,256]{1,0:T(8,128)(2,1)S(1)} %fusion.7), channel_id=2, replica_groups=mesh['grp'=2,'dp'=2,'kv'=4,'tp'=2] {'kv','tp'}, dimensions={0}, use_global_device_ids=true | all-gather | bytes 36864 | tf_op jit(solution)/shard_map/all_gather | solution.py:121
  99.6 0.1 multiply_reduce_fusion
  99.8 5.3 %convolution_convert_fusion = bf16[8,2048]{1,0:T(8,128)(2,1)} fusion(bf16[1024,2048]{1,0:T(8,128)(2,1)} %param.31, bf16[2048,1024]{1,0:T(8,128)(2,1)} %param.30, f32[8,2048]{1,0:T(8,128)S(1)} %bitcast.87, f32[2048]{0:T(1024)S(1)} %copy-done.4, f32[8]{0:T(128)S(1)} %add_rsqrt_fusion), kind=kOutput, calls=%fused_computation | convolution fusion | flops 67190784 | bytes 8495136 | tf_op jit(solution)/shard_map/dot_general | solution.py:126
  105.1 28.9 %reduce-scatter.2.cloned.1.call-done = bf16[8,256]{1,0:T(8,128)(2,1)} async-done(((bf16[8,2048]{1,0:T(8,128)(2,1)}), bf16[8,256]{1,0:T(8,128)(2,1)}) %reduce-scatter.2.cloned.1.call-update) | async-done | bytes 4112 | tf_op jit(solution)/shard_map/reduce_scatter | solution.py:127
  134.0 1.3 add_convert_fusion
  (34 shorter events, 1.0 us)
Async XLA Ops:
  7.2 78.2 %copy-start = (bf16[1536,256]{1,0:T(8,128)(2,1)S(1)}, bf16[1536,256]{1,0:T(8,128)(2,1)}, u32[]{:S(2)}) copy-start(bf16[1536,256]{1,0:T(8,128)(2,1)} %param.28) | copy-start | bytes 2359300
  7.2 78.2 %copy-start.3 = (bf16[8,256]{1,0:T(8,128)(2,1)S(1)}, bf16[8,256]{1,0:T(8,128)(2,1)}, u32[]{:S(2)}) copy-start(bf16[8,256]{1,0:T(8,128)(2,1)} %param.16) | copy-start | bytes 12292
  7.2 62.3 %copy-start.1 = (f32[1,12,16384]{2,0,1:T(1,128)S(1)}, f32[1,12,16384]{2,0,1:T(1,128)}, u32[]{:S(2)}) copy-start(f32[1,12,16384]{2,0,1:T(1,128)} %param.17) | copy-start | bytes 2359300
  7.2 64.0 %copy-start.5 = (f32[128]{0:T(128)S(1)}, f32[128]{0:T(128)}, u32[]{:S(2)}) copy-start(f32[128]{0:T(128)} %param.27) | copy-start | bytes 1540
  7.2 92.6 %copy-start.4 = (f32[2048]{0:T(1024)S(1)}, f32[2048]{0:T(1024)}, u32[]{:S(2)}) copy-start(f32[2048]{0:T(1024)} %param.29) | copy-start | bytes 24580
  26.2 14.7 %all-to-all-start.1 = ((bf16[8,1,192]{2,1,0:T(2,128)(2,1)}), bf16[8,1,192]{2,1,0:T(2,128)(2,1)S(1)}, u32[]{:S(2)}, u32[]{:S(2)}) async-start(bf16[8,1,192]{2,1,0:T(2,128)(2,1)} %copy.23), calls=%async_computation.1 | async-start | bytes 16384 | tf_op jit(solution)/shard_map/all_to_all | solution.py:103
  40.9 10.7 %all-to-all-start.3 = ((bf16[8,1,192]{2,1,0:T(2,128)(2,1)}), bf16[8,1,192]{2,1,0:T(2,128)(2,1)S(1)}, u32[]{:S(2)}, u32[]{:S(2)}) async-start(bf16[8,1,192]{2,1,0:T(2,128)(2,1)} %copy.25), calls=%async_computation.3 | async-start | bytes 16384 | tf_op jit(solution)/shard_map/all_to_all | solution.py:103
  51.6 8.9 %all-to-all-start = ((bf16[8,1,192]{2,1,0:T(2,128)(2,1)}), bf16[8,1,192]{2,1,0:T(2,128)(2,1)S(1)}, u32[]{:S(2)}, u32[]{:S(2)}) async-start(bf16[8,1,192]{2,1,0:T(2,128)(2,1)} %copy.22), calls=%async_computation | async-start | bytes 16384 | tf_op jit(solution)/shard_map/all_to_all | solution.py:103
  60.5 8.9 %all-to-all-start.2 = ((bf16[8,1,192]{2,1,0:T(2,128)(2,1)}), bf16[8,1,192]{2,1,0:T(2,128)(2,1)S(1)}, u32[]{:S(2)}, u32[]{:S(2)}) async-start(bf16[8,1,192]{2,1,0:T(2,128)(2,1)} %copy.24), calls=%async_computation.2 | async-start | bytes 16384 | tf_op jit(solution)/shard_map/all_to_all | solution.py:103
  63.8 70.2 %reduce-scatter.2.cloned.1.call-start = ((), (), s32[]{:S(2)}) async-start(), calls=%async_computation.5 | async-start | bytes 36864 | tf_op jit(solution)/shard_map/reduce_scatter | solution.py:127
  70.6 34.5 %copy-start.2 = (f32[12,128,128]{2,1,0:T(8,128)}, f32[12,128,128]{2,1,0:T(8,128)S(1)}, u32[]{:S(2)}) copy-start(f32[12,128,128]{2,1,0:T(8,128)S(1)} %multiply_add_fusion) | copy-start | bytes 2359300
Sparse Core Ops, SparseCore 0:
  105.2 28.7 reduce-scatter.1
